TPU v7x, 32 devices: a whole 2x2x4 slice. The times are simulated.
32 devices in a mesh: ep: 8 (over z, y), tp: 4 (over x, core).
Axes of the slice: x: 2, y: 2, z: 4, core: 2. Of those that a mesh axis runs over, the one named last changes fastest.
Arguments:
- value_in: bfloat16 [4096, 2048], P('ep', 'tp'), may hold values from -400 to 400
- gate_in: bfloat16 [4096, 2048], P('ep', 'tp'), may hold values from -8 to 8
- conv_taps: float32 [31, 2048], P(None, 'tp'), may hold values from -1 to 1
- conv_bias: float32 [2048], P('tp'), may hold values from -3 to 3
- ln_gain: float32 [2048], P('tp'), may hold values from 0.1 to 1.9
- ln_bias: float32 [2048], P('tp'), may hold values from -3 to 3
- out_proj: bfloat16 [2048, 4096], P('tp'), may hold values from -0.125 to 0.125
- tokens_b: bfloat16 [4096, 4096], P('ep'), may hold values from -6 to 6
- norm_gain: float32 [4096], replicated, may hold values from 0.1 to 1.9
- routes: int32 [4096, 2], P(('ep', 'tp')), may hold values from 0 to 7, all different within a row; in each aligned block of 128 rows (0 to 127, 128 to 255, ...) at most 48 rows name the same one
- route_weights: float32 [4096, 2], P(('ep', 'tp')), may hold values from 0.2 to 1.5
- expert_gate: bfloat16 [8, 4096, 1024], P('ep', None, 'tp'), may hold values from -0.09375 to 0.09375
- expert_up: bfloat16 [8, 4096, 1024], P('ep', None, 'tp'), may hold values from -0.09375 to 0.09375
- expert_down: bfloat16 [8, 1024, 4096], P('ep', 'tp'), may hold values from -0.1875 to 0.1875
- shared_gate: bfloat16 [4096, 1024], P(None, 'tp'), may hold values from -0.09375 to 0.09375
- shared_up: bfloat16 [4096, 1024], P(None, 'tp'), may hold values from -0.09375 to 0.09375
- shared_down: bfloat16 [1024, 4096], P('tp'), may hold values from -0.1875 to 0.1875
Outputs:
- mixer_out: bfloat16 [4096, 4096], P(('ep', 'tp'))
- experts_out: bfloat16 [4096, 4096], P(('ep', 'tp'))
Inputs may be any that keep to these rules, and one draw needn't show every extreme that they name: `routes`: each row names 2 different experts. In each aligned block of 128 rows (the rows of one device) no expert is named by more than 48 rows, and in some blocks an expert is named by exactly 48 rows.
All inputs are finite; a program needn't handle non-finite values.
Results may differ from a plain program's by a relative error of at most 0.012.
Values may be sent and summed in bfloat16 or wider, within the bound.
A program may use at most 128 MiB of HBM per device.

v0:
```python
import jax
import jax.numpy as jnp
from jax import lax
from jax.sharding import PartitionSpec as P

EPSILON = 1e-06


def shifted(x, axis, by):
    devices = lax.axis_size(axis)
    pairs = [(i, i + by) for i in range(devices) if 0 <= i + by < devices]
    return lax.ppermute(x, axis, pairs)


def slot_table(route_ids, expert_count):
    chosen = route_ids.reshape(-1)
    onehot = (chosen[:, None] == jnp.arange(expert_count, dtype=jnp.int32)[None, :]).astype(
        jnp.int32
    )
    earlier = jnp.cumsum(onehot, axis=0) - onehot
    return (chosen, jnp.sum(earlier * onehot, axis=1))


def gated_hidden(rows_in, weight_gate, weight_up):
    row_shape = rows_in.shape
    matrix = rows_in.reshape(-1, row_shape[-1])
    hidden = (
        jax.nn.silu(jnp.dot(matrix, weight_gate, preferred_element_type=jnp.float32))
        * jnp.dot(matrix, weight_up, preferred_element_type=jnp.float32)
    ).astype(jnp.bfloat16)
    return hidden.reshape(row_shape[:-1] + (weight_gate.shape[1],))


def project_down(hidden, weight):
    row_shape = hidden.shape
    product = jnp.dot(hidden.reshape(-1, row_shape[-1]), weight, preferred_element_type=jnp.float32)
    return product.reshape(row_shape[:-1] + (weight.shape[1],))


def per_device(
    value_in,
    gate_in,
    conv_taps,
    conv_bias,
    ln_gain,
    ln_bias,
    out_proj,
    tokens_b,
    norm_gain,
    routes,
    route_weights,
    expert_gate,
    expert_up,
    expert_down,
    shared_gate,
    shared_up,
    shared_down,
):
    tp_count = lax.axis_size("tp")
    ep_count = lax.axis_size("ep")
    gated = (value_in.astype(jnp.float32) * jax.nn.sigmoid(gate_in.astype(jnp.float32))).astype(
        jnp.bfloat16
    )
    rim_rows = conv_taps.shape[0] - 1
    length = gated.shape[0]
    before = shifted(gated[length - rim_rows :], "ep", 1)
    padded = jnp.concatenate([before, gated], axis=0).astype(jnp.float32)
    filtered = jnp.zeros(gated.shape, jnp.float32) + conv_bias[None, :]
    for tap_index in range(rim_rows + 1):
        filtered = filtered + conv_taps[tap_index][None, :] * padded[tap_index : tap_index + length]
    row_sum, squares = lax.psum(
        (jnp.sum(filtered, axis=1), jnp.sum(filtered * filtered, axis=1)), "tp"
    )
    channel_count = filtered.shape[1] * tp_count
    average = row_sum / channel_count
    variance = squares / channel_count - average * average
    normed_a = (filtered - average[:, None]) * lax.rsqrt(
        variance[:, None] + EPSILON
    ) * ln_gain + ln_bias
    activated = jax.nn.silu(normed_a).astype(jnp.bfloat16)
    features = tokens_b.astype(jnp.float32)
    normed_b = (
        features
        * lax.rsqrt(jnp.mean(features * features, axis=1, keepdims=True) + EPSILON)
        * norm_gain
    ).astype(jnp.bfloat16)
    rows_own, top_count = routes.shape
    model_width = normed_b.shape[1]
    own_rows = lax.dynamic_slice_in_dim(normed_b, lax.axis_index("tp") * rows_own, rows_own, 0)
    capacity = max(2, 3 * rows_own * top_count // (2 * ep_count))
    chosen, places = slot_table(routes, ep_count)
    source = jnp.repeat(own_rows, top_count, axis=0)
    outbox = (
        jnp.zeros((ep_count, capacity, model_width), jnp.bfloat16).at[chosen, places].set(source)
    )
    gate_local = expert_gate[0]
    up_local = expert_up[0]
    down_local = expert_down[0]
    arrived = lax.all_to_all(outbox, "ep", split_axis=0, concat_axis=0, tiled=True)
    hidden_routed = gated_hidden(
        lax.all_gather(arrived[None], "tp", axis=0, tiled=True), gate_local, up_local
    )
    hidden_routed = hidden_routed.reshape(tp_count, ep_count * capacity, -1)
    hidden_shared = gated_hidden(normed_b, shared_gate, shared_up).reshape(tp_count, rows_own, -1)
    mixer_rows = lax.psum_scatter(
        jnp.dot(activated, out_proj, preferred_element_type=jnp.float32).astype(jnp.bfloat16),
        "tp",
        scatter_dimension=0,
        tiled=True,
    )
    summed = lax.psum_scatter(
        jnp.concatenate(
            [project_down(hidden_routed, down_local), project_down(hidden_shared, shared_down)],
            axis=1,
        ).astype(jnp.bfloat16),
        "tp",
        scatter_dimension=0,
        tiled=True,
    ).astype(jnp.float32)[0]
    summed = summed.astype(jnp.bfloat16)
    routed_rows = summed[: ep_count * capacity].reshape(ep_count, capacity, model_width)
    shared_rows = summed[ep_count * capacity :]
    returned = lax.all_to_all(routed_rows, "ep", split_axis=0, concat_axis=0, tiled=True)
    picked = returned[chosen, places].astype(jnp.float32) * route_weights.reshape(-1)[:, None]
    experts_out = (
        shared_rows.astype(jnp.float32)
        + jnp.sum(picked.reshape(rows_own, top_count, model_width), axis=1)
    ).astype(jnp.bfloat16)
    return (mixer_rows, experts_out)


def solution(mesh):
    return jax.shard_map(
        per_device,
        mesh=mesh,
        in_specs=(
            P("ep", "tp"),
            P("ep", "tp"),
            P(None, "tp"),
            P("tp"),
            P("tp"),
            P("tp"),
            P("tp", None),
            P("ep", None),
            P(),
            P(("ep", "tp"), None),
            P(("ep", "tp"), None),
            P("ep", None, "tp"),
            P("ep", None, "tp"),
            P("ep", "tp", None),
            P(None, "tp"),
            P(None, "tp"),
            P("tp", None),
        ),
        out_specs=(P(("ep", "tp"), None), P(("ep", "tp"), None)),
        check_vma=False,
    )
```

profile of v0, /device:TPU:0, one launch (start us, length us, event | category | flops | bytes accessed | tf_op | source)
XLA Modules:
  0.0 520.9 jit_solution(433800044017684234)
XLA Ops:
  9.4 3.1 fusion
  12.5 3.8 fusion.2
  18.5 3.5 broadcast_in_dim.7
  21.9 4.1 reshape.128
  28.2 67.2 %scatter_fusion = bf16[8,48,4096]{2,1,0:T(8,128)(2,1)} fusion(bf16[8,48,4096]{2,1,0:T(8,128)(2,1)} %broadcast_in_dim.6, s32[256]{0:T(256)S(1)} %bitcast.71, bf16[256,4096]{1,0:T(8,128)(2,1)} %reshape.128), kind=kCustom, calls=%fused_computation.1 | custom fusion | bytes 6293504 | tf_op jit(solution)/shard_map/scatter | solution.py:94
  95.4 78.3 %all_to_all.10 = bf16[8,48,4096]{2,1,0:T(8,128)(2,1)} all-to-all(bf16[8,48,4096]{2,1,0:T(8,128)(2,1)} %scatter_fusion), channel_id=1, replica_groups=mesh['ep'=8,'tp'=4] {'ep'}, dimensions={0} | all-to-all | bytes 6291456 | tf_op jit(solution)/shard_map/all_to_all | solution.py:99
  173.9 4.1 fusion.63
  178.0 11.1 %convolution_convert_fusion.1 = bf16[512,4096]{1,0:T(8,128)(2,1)} fusion(bf16[256,4096]{1,0:T(8,128)(2,1)} %param.33, bf16[512,4096]{1,0:T(8,128)(2,1)} %copy-done.2, bf16[4096,256]{1,0:T(8,128)(2,1)} %param.32, f32[512,256]{1,0:T(8,128)S(1)} %fusion.63), kind=kOutput, calls=%fused_computation.9 | convolution fusion | flops 2150367232 | bytes 13107200 | tf_op jit(solution)/shard_map/dot_general | solution.py:36
  189.1 65.5 %all-gather.3.cloned.1.call-done = bf16[32,48,4096]{2,1,0:T(8,128)(2,1)} async-done(((bf16[8,48,4096]{2,1,0:T(8,128)(2,1)}), bf16[32,48,4096]{2,1,0:T(8,128)(2,1)}) %all-gather.3.cloned.1.call-update) | async-done | bytes 12582928 | tf_op jit(solution)/shard_map/all_gather | solution.py:101
  254.6 7.7 %fusion.7 = f32[1536,256]{1,0:T(8,128)S(1)} fusion(bf16[1536,4096]{1,0:T(8,128)(2,1)} %bitcast.107, bf16[1,4096,256]{2,1,0:T(8,128)(2,1)} %param.28), kind=kOutput, calls=%fused_computation.18 | convolution fusion | flops 3221225472 | bytes 16252928 | tf_op jit(solution)/shard_map/dot_general | solution.py:28
  264.0 3.9 fusion.3
  267.9 6.4 %convolution_convert_fusion = bf16[4,384,4096]{2,1,0:T(8,128)(2,1)} fusion(bf16[4,384,256]{2,1,0:T(8,128)(2,1)S(1)} %bitcast.74, bf16[1,256,4096]{2,1,0:T(8,128)(2,1)S(1)} %copy-done), kind=kOutput, calls=%fused_computation.5 | convolution fusion | flops 3227516928 | bytes 15466496 | tf_op jit(solution)/shard_map/dot_general | solution.py:36
  274.3 12.4 %pad_maximum_fusion = bf16[4,512,4096]{2,1,0:T(8,128)(2,1)} fusion(bf16[4,128,4096]{2,1,0:T(8,128)(2,1)S(1)} %bitcast.73, bf16[4,384,4096]{2,1,0:T(8,128)(2,1)} %convolution_convert_fusion), kind=kLoop, calls=%fused_computation.2 | loop fusion | flops 33554432 | bytes 33554432 | tf_op jit(solution)/shard_map/concatenate | solution.py:112
  288.3 3.6 collective-permute-start
  293.4 5.0 fusion.58
  298.4 6.0 %all-reduce = (f32[512]{0:T(512)S(1)}, f32[512]{0:T(512)S(1)}) all-reduce(f32[512]{0:T(512)S(1)} %get-tuple-element.3, f32[512]{0:T(512)S(1)} %get-tuple-element.2), channel_id=1, replica_groups=mesh['ep'=8,'tp'=4] {'tp'}, use_global_device_ids=true, to_apply=%region_3.0 | all-reduce | flops 1024 | bytes 8192 | tf_op jit(solution)/shard_map/psum | solution.py:71
  304.4 7.9 %convolution_convert_fusion.2 = bf16[512,4096]{1,0:T(8,128)(2,1)} fusion(bf16[512,4096]{1,0:T(8,128)(2,1)} %param.23, f32[512,512]{1,0:T(8,128)S(1)} %get-tuple-element.8, f32[512]{0:T(512)S(1)} %copy-done.13, f32[512]{0:T(512)S(1)} %copy-done.14, f32[512]{0:T(512)S(1)} %get-tuple-element.41, f32[512]{0:T(512)S(1)} %get-tuple-element.40), kind=kOutput, calls=%fused_computation.10 | convolution fusion | flops 2151940096 | bytes 9445376 | tf_op jit(solution)/shard_map/dot_general | solution.py:106
  312.3 99.7 %reduce-scatter.5.cloned.1.call-done = bf16[1,512,4096]{2,1,0:T(8,128)(2,1)} async-done(((bf16[4,512,4096]{2,1,0:T(8,128)(2,1)}), bf16[1,512,4096]{2,1,0:T(8,128)(2,1)}) %reduce-scatter.5.cloned.1.call-update) | async-done | bytes 4194320 | tf_op jit(solution)/shard_map/reduce_scatter | solution.py:111
  412.0 3.9 slice.308
  415.9 5.6 %all-to-all-start.1 = ((bf16[8,48,4096]{2,1,0:T(8,128)(2,1)}), bf16[8,48,4096]{2,1,0:T(8,128)(2,1)}, u32[]{:S(2)}, u32[]{:S(2)}) async-start(bf16[8,48,4096]{2,1,0:T(8,128)(2,1)} %bitcast.72), calls=%async_computation.3 | async-start | bytes 6291456 | tf_op jit(solution)/shard_map/all_to_all | solution.py:123
  421.7 70.5 %all-to-all-done.1 = bf16[8,48,4096]{2,1,0:T(8,128)(2,1)} async-done(((bf16[8,48,4096]{2,1,0:T(8,128)(2,1)}), bf16[8,48,4096]{2,1,0:T(8,128)(2,1)}, u32[]{:S(2)}, u32[]{:S(2)}) %all-to-all-start.1) | async-done | bytes 3145760 | tf_op jit(solution)/shard_map/all_to_all | solution.py:123
  492.3 6.0 %gather_fusion = bf16[256,4096]{1,0:T(8,128)(2,1)S(1)} fusion(bf16[8,48,4096]{2,1,0:T(8,128)(2,1)} %all-to-all-done.1, s32[256]{0:T(256)S(1)} %bitcast.70), kind=kCustom, calls=%fused_computation | custom fusion | bytes 4196352 | tf_op jit(solution)/shard_map/gather | solution.py:124
  498.3 4.2 reshape.119
  502.5 8.9 %multiply_reduce_fusion = f32[128,4096]{1,0:T(8,128)S(1)} fusion(f32[128,2,4096]{2,1,0:T(2,128)} %reshape.119, f32[128,2]{1,0:T(8,128)S(1)} %copy.27), kind=kLoop, calls=%fused_computation.11 | loop fusion | flops 1572864 | bytes 6292480 | tf_op jit(solution)/shard_map/reduce_sum | solution.py:127
  (61 shorter events, 13.9 us)
Async XLA Ops:
  7.2 260.7 %copy-start = (bf16[1,256,4096]{2,1,0:T(8,128)(2,1)S(1)}, bf16[1,256,4096]{2,1,0:T(8,128)(2,1)}, u32[]{:S(2)}) copy-start(bf16[1,256,4096]{2,1,0:T(8,128)(2,1)} %param.30) | copy-start | bytes 6291460
  7.2 5.4 %copy-start.7 = (f32[4096]{0:T(1024)S(1)}, f32[4096]{0:T(1024)}, u32[]{:S(2)}) copy-start(f32[4096]{0:T(1024)} %param.25) | copy-start | bytes 49156
  7.2 247.4 %all-gather.3.cloned.1.call-start = ((), (), s32[]{:S(2)}) async-start(), calls=%async_computation.6 | async-start | bytes 15728640 | tf_op jit(solution)/shard_map/all_gather | solution.py:101
  9.4 6.9 %copy-start.8 = (s32[8,3]{0,1:T(4,128)}, s32[8,3]{0,1:T(4,128)S(1)}, u32[]{:S(2)}) copy-start(s32[8,3]{0,1:T(4,128)S(1)} %reduce-window.9) | copy-start | bytes 292
  16.4 2.0 copy-start.2
  18.4 7.6 %slice-start = ((s32[8,3]{0,1:T(4,128)}), s32[8,2]{0,1:T(2,128)S(1)}, s32[]{:S(2)}) async-start(s32[8,3]{0,1:T(4,128)} %copy-done.8), calls=%async_computation.7 | async-start | bytes 2048 | tf_op jit(solution)/shard_map/slice.1
  173.7 238.3 %reduce-scatter.5.cloned.1.call-start = ((), (), s32[]{:S(2)}) async-start(), calls=%async_computation.5 | async-start | bytes 20971520 | tf_op jit(solution)/shard_map/reduce_scatter | solution.py:111
  254.6 8.8 %copy-start.11 = (bf16[32,48,4096]{2,1,0:T(8,128)(2,1)S(1)}, bf16[32,48,4096]{2,1,0:T(8,128)(2,1)}, u32[]{:S(2)}) copy-start(bf16[32,48,4096]{2,1,0:T(8,128)(2,1)} %all-gather.3.cloned.1.call-done) | copy-start | bytes 37748740
  254.6 9.4 %copy-start.12 = (bf16[1,4096,256]{2,1,0:T(8,128)(2,1)S(1)}, bf16[1,4096,256]{2,1,0:T(8,128)(2,1)}, u32[]{:S(2)}) copy-start(bf16[1,4096,256]{2,1,0:T(8,128)(2,1)} %param.29) | copy-start | bytes 6291460
  267.9 6.4 %copy-start.3 = (bf16[512,4096]{1,0:T(8,128)(2,1)S(1)}, bf16[512,4096]{1,0:T(8,128)(2,1)}, u32[]{:S(2)}) copy-start(bf16[512,4096]{1,0:T(8,128)(2,1)} %convolution_convert_fusion.1) | copy-start | bytes 12582916
  286.8 1.0 copy-start.4
  286.8 1.2 copy-start.5
  286.8 5.1 copy-start.6
  286.8 6.6 %copy-start.9 = (f32[512]{0:T(512)S(1)}, f32[512]{0:T(512)}, u32[]{:S(2)}) copy-start(f32[512]{0:T(512)} %param.20) | copy-start | bytes 6148
  286.8 227.1 %reduce-scatter.3.cloned.1.call-start = ((), (), s32[]{:S(2)}) async-start(), calls=%async_computation.4 | async-start | bytes 5242880 | tf_op jit(solution)/shard_map/reduce_scatter | solution.py:105
  288.3 5.0 collective-permute-start
  293.4 11.0 %copy-start.13 = (f32[512]{0:T(512)S(1)}, f32[512]{0:T(512)}, u32[]{:S(2)}) copy-start(f32[512]{0:T(512)} %param.22) | copy-start | bytes 6148
  293.4 11.0 %copy-start.14 = (f32[512]{0:T(512)S(1)}, f32[512]{0:T(512)}, u32[]{:S(2)}) copy-start(f32[512]{0:T(512)} %param.21) | copy-start | bytes 6148
  415.9 5.7 %copy-start.10 = (f32[128,2]{0,1:T(2,128)S(1)}, f32[128,2]{0,1:T(2,128)}, u32[]{:S(2)}) copy-start(f32[128,2]{0,1:T(2,128)} %param.27) | copy-start | bytes 3076
  415.9 76.3 %all-to-all-start.1 = ((bf16[8,48,4096]{2,1,0:T(8,128)(2,1)}), bf16[8,48,4096]{2,1,0:T(8,128)(2,1)}, u32[]{:S(2)}, u32[]{:S(2)}) async-start(bf16[8,48,4096]{2,1,0:T(8,128)(2,1)} %bitcast.72), calls=%async_computation.3 | async-start | bytes 6291456 | tf_op jit(solution)/shard_map/all_to_all | solution.py:123
  502.5 11.3 %copy-start.1 = (bf16[1,256,4096]{2,1,0:T(8,128)(2,1)S(1)}, bf16[1,256,4096]{2,1,0:T(8,128)(2,1)}, u32[]{:S(2)}) copy-start(bf16[1,256,4096]{2,1,0:T(8,128)(2,1)} %param.30) | copy-start | bytes 6291460
Sparse Core Ops, SparseCore 0:
  173.8 80.7 all-gather.2
  286.9 125.0 reduce-scatter.4
  415.1 44.5 reduce-scatter.2
where the time goes:
time: 527 us; the launch traced here: 521 us
  waiting for transfers between devices  237 us (45%)
  local copies, waits for them, and re-layouts  97.6 us (19%)
  blocking collectives  84.2 us (16%)
  matrix products  41.2 us (8%)
  other arithmetic  36.9 us (7%)
  between operations  14.4 us (3%)
  starting transfers between devices  9.53 us (2%)
    reduce_scatter x1, waiting for transfers between devices, per_device(): lax.psum_scatter(jnp.concatenate([project_down(hidden_routed, down_local)...  99.7 us
    all_to_all x1, blocking collectives, per_device(): lax.all_to_all(outbox, 'ep', split_axis=0, concat_axis=0, tiled=True)  78.3 us
    all_to_all x1, waiting for transfers between devices, per_device(): lax.all_to_all(routed_rows, 'ep', split_axis=0, concat_axis=0, tiled=True)  70.5 us
    scatter x1, local copies, waits for them, and re-layouts, per_device(): jnp.zeros((ep_count, capacity, model_width), jnp.bfloat16)  67.2 us
    all_gather x1, waiting for transfers between devices, per_device(): lax.all_gather(arrived[None], 'tp', axis=0, tiled=True)  65.5 us
    dot_general x2, matrix products, project_down(): jnp.dot(hidden.reshape(-1, row_shape[-1]), weight, preferred_element_type...  17.5 us
    concatenate x1, other arithmetic, per_device(): jnp.concatenate([project_down(hidden_routed, down_local), project_down(hi...  12.4 us
    dot_general x2, matrix products, gated_hidden(): jnp.dot(matrix, weight_gate, preferred_element_type=jnp.float32)  11.8 us
  transfers between devices with their start and end apart: 5, of which 4 were waited for; matrix products, arithmetic and copies ran while one was open for 10% of the time, Pallas kernels for 0%

commit v1 on v0

v1 whole, which is shorter than its diff:
```python
import jax
import jax.numpy as jnp
from jax import lax
from jax.sharding import PartitionSpec as P

EPSILON = 1e-06
COLUMN_CHUNKS = 2


def shifted(x, axis, by):
    devices = lax.axis_size(axis)
    pairs = [(i, i + by) for i in range(devices) if 0 <= i + by < devices]
    return lax.ppermute(x, axis, pairs)


def swapped(x, axis, bit):
    devices = lax.axis_size(axis)
    return lax.ppermute(x, axis, [(i, i ^ bit) for i in range(devices)])


def stages(axis):
    bits, bit = [], 1
    while bit < lax.axis_size(axis):
        bits.append(bit)
        bit *= 2
    return bits


def gathered(x, axis):
    pieces = [x]
    for bit in reversed(stages(axis)):
        pieces = pieces + [swapped(piece, axis, bit) for piece in pieces]
    return pieces


def scattered_product(lhs, weight, axis):
    count = lax.axis_size(axis)
    me = lax.axis_index(axis)
    bits = stages(axis)
    rows = lhs.shape[0] // count
    width = weight.shape[1]
    near = bits[0]
    core = me % 2
    blocks = lhs.reshape(count // 2, 2, rows, lhs.shape[1])
    sent = lax.dynamic_index_in_dim(blocks, 1 - core, 1, keepdims=False).reshape(-1, lhs.shape[1])
    kept = lax.dynamic_index_in_dim(blocks, core, 1, keepdims=False).reshape(-1, lhs.shape[1])
    sent = jnp.dot(sent, weight, preferred_element_type=jnp.float32).astype(jnp.bfloat16)
    arrived = swapped(sent, axis, near)
    kept = jnp.dot(kept, weight, preferred_element_type=jnp.float32).astype(jnp.bfloat16)
    total = (kept, arrived)
    left = count // 2
    for bit in bits[1:]:
        low = (me // bit) % 2
        halves = [part.reshape(left // 2, 2, rows, width) for part in total]
        give = [lax.dynamic_index_in_dim(h, 1 - low, 1, keepdims=False) for h in halves]
        keep = [lax.dynamic_index_in_dim(h, low, 1, keepdims=False) for h in halves]
        give = sum(g.astype(jnp.float32) for g in give).astype(jnp.bfloat16)
        total = tuple(keep) + (swapped(give, axis, bit),)
        left = left // 2
    return sum(part.reshape(rows, width).astype(jnp.float32) for part in total)


def rms_normed(features, gain):
    features = features.astype(jnp.float32)
    return (
        features
        * lax.rsqrt(jnp.mean(features * features, axis=1, keepdims=True) + EPSILON)
        * gain
    ).astype(jnp.bfloat16)


def gated_hidden(rows_in, weight_gate, weight_up):
    return (
        jax.nn.silu(jnp.dot(rows_in, weight_gate, preferred_element_type=jnp.float32))
        * jnp.dot(rows_in, weight_up, preferred_element_type=jnp.float32)
    ).astype(jnp.bfloat16)


def per_device(
    value_in,
    gate_in,
    conv_taps,
    conv_bias,
    ln_gain,
    ln_bias,
    out_proj,
    tokens_b,
    norm_gain,
    routes,
    route_weights,
    expert_gate,
    expert_up,
    expert_down,
    shared_gate,
    shared_up,
    shared_down,
):
    tp_count = lax.axis_size("tp")
    ep_count = lax.axis_size("ep")
    model_width = tokens_b.shape[1]
    rows_own, top_count = routes.shape
    capacity = max(2, 3 * rows_own * top_count // (2 * ep_count))

    gates = gathered(expert_gate[0], "tp")
    ups = gathered(expert_up[0], "tp")
    chunk = model_width // COLUMN_CHUNKS
    downs = [
        gathered(expert_down[0][:, c * chunk : (c + 1) * chunk], "tp")
        for c in range(COLUMN_CHUNKS)
    ]

    own = lax.dynamic_slice_in_dim(tokens_b, lax.axis_index("tp") * rows_own, rows_own, 0)
    own_rows = rms_normed(own, norm_gain)
    by_choice = routes.T
    expert_ids = jnp.arange(ep_count, dtype=jnp.int32)
    names = by_choice[:, None, :] == expert_ids[None, :, None]
    named = jnp.any(names, axis=0)
    row_ids = jnp.arange(rows_own, dtype=jnp.int32)
    before_row = (row_ids[:, None] < row_ids[None, :]).astype(jnp.bfloat16)
    earlier = jnp.dot(
        named.astype(jnp.bfloat16), before_row, preferred_element_type=jnp.float32
    ).astype(jnp.int32)
    slots = jnp.arange(capacity, dtype=jnp.int32)
    placed = earlier[:, None, :] == slots[None, :, None]
    pick = (placed & named[:, None, :]).astype(jnp.bfloat16).reshape(-1, rows_own)
    outbox = jnp.dot(pick, own_rows, preferred_element_type=jnp.float32).astype(jnp.bfloat16)
    arrived = lax.all_to_all(
        outbox.reshape(ep_count, capacity, model_width), "ep", split_axis=0, concat_axis=0, tiled=True
    ).reshape(ep_count * capacity, model_width)

    gated = (value_in.astype(jnp.float32) * jax.nn.sigmoid(gate_in.astype(jnp.float32))).astype(
        jnp.bfloat16
    )
    rim_rows = conv_taps.shape[0] - 1
    length = gated.shape[0]
    before = shifted(gated[length - rim_rows :], "ep", 1)
    padded = jnp.concatenate([before, gated], axis=0).astype(jnp.float32)
    filtered = jnp.zeros(gated.shape, jnp.float32) + conv_bias[None, :]
    for tap_index in range(rim_rows + 1):
        filtered = filtered + conv_taps[tap_index][None, :] * padded[tap_index : tap_index + length]
    row_sum, squares = lax.psum(
        (jnp.sum(filtered, axis=1), jnp.sum(filtered * filtered, axis=1)), "tp"
    )
    channel_count = filtered.shape[1] * tp_count
    average = row_sum / channel_count
    variance = squares / channel_count - average * average
    normed_a = (filtered - average[:, None]) * lax.rsqrt(
        variance[:, None] + EPSILON
    ) * ln_gain + ln_bias
    activated = jax.nn.silu(normed_a).astype(jnp.bfloat16)
    mixer_rows = scattered_product(activated, out_proj, "tp").astype(jnp.bfloat16)

    normed_b = rms_normed(tokens_b, norm_gain)
    hidden_shared = gated_hidden(normed_b, shared_gate, shared_up)
    shared_rows = scattered_product(hidden_shared, shared_down, "tp").astype(jnp.bfloat16)

    hidden = [gated_hidden(arrived, g, u) for g, u in zip(gates, ups)]
    parts = []
    for pieces in downs:
        product = sum(
            jnp.dot(h, piece, preferred_element_type=jnp.float32)
            for h, piece in zip(hidden, pieces)
        ).astype(jnp.bfloat16)
        parts.append(
            lax.all_to_all(
                product.reshape(ep_count, capacity, chunk),
                "ep",
                split_axis=0,
                concat_axis=0,
                tiled=True,
            ).reshape(ep_count * capacity, chunk)
        )
    outs = []
    for c, returned in enumerate(parts):
        total = shared_rows[:, c * chunk : (c + 1) * chunk].astype(jnp.float32)
        for k in range(top_count):
            choice = (placed & names[k][:, None, :]).astype(jnp.bfloat16).reshape(-1, rows_own)
            picked = lax.dot_general(
                choice, returned, (((0,), (0,)), ((), ())), preferred_element_type=jnp.float32
            )
            total = total + picked * route_weights[:, k][:, None]
        outs.append(total.astype(jnp.bfloat16))
    return (mixer_rows, jnp.concatenate(outs, axis=1))


def solution(mesh):
    return jax.shard_map(
        per_device,
        mesh=mesh,
        in_specs=(
            P("ep", "tp"),
            P("ep", "tp"),
            P(None, "tp"),
            P("tp"),
            P("tp"),
            P("tp"),
            P("tp", None),
            P("ep", None),
            P(),
            P(("ep", "tp"), None),
            P(("ep", "tp"), None),
            P("ep", None, "tp"),
            P("ep", None, "tp"),
            P("ep", "tp", None),
            P(None, "tp"),
            P(None, "tp"),
            P("tp", None),
        ),
        out_specs=(P(("ep", "tp"), None), P(("ep", "tp"), None)),
        check_vma=False,
    )
```

time: 527 us -> 246 us (0.47)
  waiting for transfers between devices: 237 us -> 51.6 us
  local copies, waits for them, and re-layouts: 97.6 us -> 2.29 us
  matrix products: 41.2 us -> 65.6 us
  starting transfers between devices: 9.53 us -> 31.2 us
  blocking collectives: 84.2 us -> 69.6 us
  other arithmetic: 36.9 us -> 23.2 us
  between operations: 14.4 us -> 1.2 us
    reduce_scatter x2 -> x0, waiting for transfers between devices: 99.7 us -> none  [the longest x1 99.7 us: per_device(): lax.psum_scatter(jnp.concatenate([project_down(hidden_routed, down_local)...]
    all_to_all x1 -> x0, blocking collectives: 78.3 us -> none  [per_device(): lax.all_to_all(outbox, 'ep', split_axis=0, concat_axis=0, tiled=True)]
    scatter x1 -> x0, local copies, waits for them, and re-layouts: 67.2 us -> none  [per_device(): jnp.zeros((ep_count, capacity, model_width), jnp.bfloat16)]
    all_gather x1 -> x0, waiting for transfers between devices: 65.5 us -> none  [per_device(): lax.all_gather(arrived[None], 'tp', axis=0, tiled=True)]
    psum x1, blocking collectives: 5.95 us -> 69.6 us  [per_device(): lax.psum((jnp.sum(filtered, axis=1), jnp.sum(filtered * filtered, axis=1)...]
    all_to_all x1 -> x3, waiting for transfers between devices: 70.5 us -> 24.9 us  [the longest x2 24.9 us: per_device(): lax.all_to_all(product.reshape(ep_count, capacity, chunk), 'ep', split_ax...]
    dot_general x6 -> x28, matrix products: 41.2 us -> 65.6 us  [the longest x5 18.5 us: gated_hidden(): jnp.dot(rows_in, weight_gate, preferred_element_type=jnp.float32)]
    ppermute x0 -> x16, waiting for transfers between devices: none -> 20.5 us  [swapped(): return lax.ppermute(x, axis, [(i, i ^ bit) for i in range(devices)])]
  transfers between devices with their start and end apart: 5 -> 20, of which waited for: 4 -> 4; matrix products, arithmetic and copies ran while one was open for 10% -> 35% of each run, Pallas kernels for 0% -> 0%
where the time goes in v1:
time: 246 us; the launch traced here: 245 us
  blocking collectives  69.6 us (28%)
  matrix products  65.6 us (27%)
  waiting for transfers between devices  51.6 us (21%)
  starting transfers between devices  31.2 us (13%)
  other arithmetic  23.2 us (9%)
    psum x1, blocking collectives, per_device(): lax.psum((jnp.sum(filtered, axis=1), jnp.sum(filtered * filtered, axis=1)...  69.6 us
    all_to_all x2, waiting for transfers between devices, per_device(): lax.all_to_all(product.reshape(ep_count, capacity, chunk), 'ep', split_ax...  24.9 us
    ppermute x16, waiting for transfers between devices, swapped(): return lax.ppermute(x, axis, [(i, i ^ bit) for i in range(devices)])  20.5 us
    dot_general x5, matrix products, gated_hidden(): jnp.dot(rows_in, weight_gate, preferred_element_type=jnp.float32)  18.5 us
    dot_general x5, matrix products, gated_hidden(): jnp.dot(rows_in, weight_up, preferred_element_type=jnp.float32)  14.3 us
    dot_general x8, matrix products, per_device(): jnp.dot(h, piece, preferred_element_type=jnp.float32)  10.9 us
    ppermute x16, starting transfers between devices, swapped(): return lax.ppermute(x, axis, [(i, i ^ bit) for i in range(devices)])  10.7 us
    all_to_all x2, starting transfers between devices, per_device(): lax.all_to_all(product.reshape(ep_count, capacity, chunk), 'ep', split_ax...  10.4 us
  transfers between devices with their start and end apart: 20, of which 4 were waited for; matrix products, arithmetic and copies ran while one was open for 35% of the time, Pallas kernels for 0%

profile of v1, /device:TPU:0, one launch (start us, length us, event | category | flops | bytes accessed | tf_op | source)
XLA Modules:
  0.0 244.8 jit_solution(1150967203151739206)
XLA Ops:
  0.6 3.0 %collective-permute-start.5 = (bf16[4096,256]{1,0:T(8,128)(2,1)}, bf16[4096,256]{1,0:T(8,128)(2,1)}, u32[]{:S(2)}, u32[]{:S(2)}) collective-permute-start(bf16[4096,256]{1,0:T(8,128)(2,1)} %bitcast.201), channel_id=1, source_target_pairs={{0,2},{1,3},{2,0},{3,1},{4,6},{5,7},{6,4},{7,5},{8,10},{9,11},{10,... | collective-permute-start | bytes 6291464 | tf_op jit(solution)/shard_map/ppermute | solution.py:18
  6.8 4.0 %convolution_convert_fusion = bf16[384,4096]{1,0:T(8,128)(2,1)} fusion(pred[384,128]{1,0:T(32,128)(4,1)S(1)} %fusion.68, f32[4096]{0:T(1024)} %param.25, f32[128]{0:T(128)S(1)} %add_rsqrt_fusion.2, bf16[512,4096]{1,0:T(8,128)(2,1)} %param.24, s32[]{:T(128)S(6)} %select_n.53), kind=kOutput, calls=%fused_computation.5 | convolution fusion | flops 406323200 | bytes 4260356 | tf_op jit(solution)/shard_map/dot_general | solution.py:126
  10.8 6.2 %all-to-all-start = ((bf16[8,48,4096]{2,1,0:T(8,128)(2,1)}), bf16[8,48,4096]{2,1,0:T(8,128)(2,1)}, u32[]{:S(2)}, u32[]{:S(2)}) async-start(bf16[8,48,4096]{2,1,0:T(8,128)(2,1)} %bitcast.153), calls=%async_computation | async-start | bytes 6291456 | tf_op jit(solution)/shard_map/all_to_all | solution.py:127
  18.4 3.9 %collective-permute-start = (bf16[30,512]{1,0:T(8,128)(2,1)S(1)}, bf16[30,512]{1,0:T(8,128)(2,1)S(1)}, u32[]{:S(2)}, u32[]{:S(2)}) collective-permute-start(bf16[30,512]{1,0:T(8,128)(2,1)S(1)} %slice.288), channel_id=1, source_target_pairs={{0,4},{4,8},{8,12},{12,16},{16,20},{20,24},{24,28},{1,5},{5,9},{9,... | collective-permute-start | bytes 92168 | tf_op jit(solution)/shard_map/ppermute | solution.py:13
  22.3 3.1 %fusion = f32[512]{0:T(512)S(1)} fusion(bf16[512,4096]{1,0:T(8,128)(2,1)} %param.24), kind=kLoop, calls=%fused_computation.2 | loop fusion | flops 6290944 | bytes 4196352 | tf_op jit(solution)/shard_map/reduce_sum | solution.py:67
  25.5 4.3 %fusion.19 = f32[512,256]{1,0:T(8,128)S(1)} fusion(bf16[4096,256]{1,0:T(8,128)(2,1)} %param.31, bf16[512,4096]{1,0:T(8,128)(2,1)} %param.24, f32[4096]{0:T(1024)S(1)} %copy-done.14, f32[512]{0:T(512)S(1)} %add_rsqrt_fusion), kind=kOutput, calls=%fused_computation.38 | convolution fusion | flops 1082130432 | bytes 6834176 | tf_op jit(solution)/shard_map/dot_general | solution.py:74
  37.3 6.2 %collective-permute-done = bf16[30,512]{1,0:T(8,128)(2,1)S(1)} collective-permute-done((bf16[30,512]{1,0:T(8,128)(2,1)S(1)}, bf16[30,512]{1,0:T(8,128)(2,1)S(1)}, u32[]{:S(2)}, u32[]{:S(2)}) %collective-permute-start) | collective-permute-done | bytes 30752 | tf_op jit(solution)/shard_map/ppermute | solution.py:13
  45.3 5.0 %fusion.86 = (f32[512]{0:T(512)S(1)}, f32[512]{0:T(512)S(1)}, f32[512,512]{1,0:T(8,128)S(1)}) fusion(f32[542,512]{1,0:T(8,128)S(1)} %maximum_convert_fusion, f32[512]{0:T(512)S(1)} %bitcast.179, f32[512]{0:T(512)S(1)} %bitcast.180, f32[512]{0:T(512)S(1)} %bitcast.182, f32[512]{0:T(512)S(1)} %bitcast.183, f32[512]{0:T(512)S(1)} %bitcast.184, ...), kind=kLoop, calls=%fused_computation.154 | loop fusion | flops 17038336 | bytes 33624064 | tf_op jit(solution)/shard_map/reduce_sum | solution.py:142
  50.2 69.6 %all-reduce = (f32[512]{0:T(512)S(1)}, f32[512]{0:T(512)S(1)}) all-reduce(f32[512]{0:T(512)S(1)} %get-tuple-element.3, f32[512]{0:T(512)S(1)} %get-tuple-element.2), channel_id=1, replica_groups=mesh['ep'=8,'tp'=4] {'tp'}, use_global_device_ids=true, to_apply=%region_3.0 | all-reduce | flops 1024 | bytes 8192 | tf_op jit(solution)/shard_map/psum | solution.py:141
  120.5 3.5 %fusion.79 = f32[384,256]{1,0:T(8,128)S(1)} fusion(bf16[384,4096]{1,0:T(8,128)(2,1)} %bitcast.52, bf16[1,4096,256]{2,1,0:T(8,128)(2,1)} %param.28), kind=kOutput, calls=%fused_computation.147 | convolution fusion | flops 805306368 | bytes 5636096 | tf_op jit(solution)/shard_map/dot_general | solution.py:74
  124.0 3.6 %fusion.91 = f32[384,256]{1,0:T(8,128)S(1)} fusion(bf16[384,4096]{1,0:T(8,128)(2,1)} %bitcast.52, bf16[4096,256]{1,0:T(8,128)(2,1)} %collective-permute-done.5), kind=kOutput, calls=%fused_computation.158 | convolution fusion | flops 805306368 | bytes 5636096 | tf_op jit(solution)/shard_map/dot_general | solution.py:74
  128.2 3.6 %fusion.93 = f32[384,256]{1,0:T(8,128)S(1)} fusion(bf16[384,4096]{1,0:T(8,128)(2,1)} %bitcast.52, bf16[4096,256]{1,0:T(8,128)(2,1)} %collective-permute-done.8), kind=kOutput, calls=%fused_computation.160 | convolution fusion | flops 805306368 | bytes 5636096 | tf_op jit(solution)/shard_map/dot_general | solution.py:74
  131.8 2.9 %fusion.24 = bf16[384,256]{1,0:T(8,128)(2,1)S(1)} fusion(bf16[384,4096]{1,0:T(8,128)(2,1)} %bitcast.52, f32[384,256]{1,0:T(8,128)S(1)} %fusion.79, bf16[1,4096,256]{2,1,0:T(8,128)(2,1)S(1)} %copy-done.21), kind=kOutput, calls=%fused_computation.41 | convolution fusion | flops 805896192 | bytes 5832704 | tf_op jit(solution)/shard_map/dot_general | solution.py:75
  135.0 3.5 %fusion.95 = f32[384,256]{1,0:T(8,128)S(1)} fusion(bf16[384,4096]{1,0:T(8,128)(2,1)} %bitcast.52, bf16[4096,256]{1,0:T(8,128)(2,1)} %collective-permute-done.11), kind=kOutput, calls=%fused_computation.162 | convolution fusion | flops 805306368 | bytes 5636096 | tf_op jit(solution)/shard_map/dot_general | solution.py:74
  138.6 3.7 %multiply_convert_fusion.4 = bf16[384,256]{1,0:T(8,128)(2,1)S(1)} fusion(f32[384,256]{1,0:T(8,128)S(1)} %fusion.91, bf16[384,4096]{1,0:T(8,128)(2,1)} %bitcast.52, bf16[4096,256]{1,0:T(8,128)(2,1)} %collective-permute-done.6), kind=kOutput, calls=%fused_computation.117 | convolution fusion | flops 805896192 | bytes 5832704 | tf_op jit(solution)/shard_map/dot_general | solution.py:75
  143.5 3.5 %multiply_convert_fusion.3 = bf16[384,256]{1,0:T(8,128)(2,1)S(1)} fusion(f32[384,256]{1,0:T(8,128)S(1)} %fusion.93, bf16[384,4096]{1,0:T(8,128)(2,1)} %bitcast.52, bf16[4096,256]{1,0:T(8,128)(2,1)} %collective-permute-done.9), kind=kOutput, calls=%fused_computation.116 | convolution fusion | flops 805896192 | bytes 5832704 | tf_op jit(solution)/shard_map/dot_general | solution.py:75
  149.9 2.9 %multiply_convert_fusion.2 = bf16[384,256]{1,0:T(8,128)(2,1)S(1)} fusion(f32[384,256]{1,0:T(8,128)S(1)} %fusion.95, bf16[384,4096]{1,0:T(8,128)(2,1)} %bitcast.52, bf16[4096,256]{1,0:T(8,128)(2,1)S(1)} %collective-permute-done.12), kind=kOutput, calls=%fused_computation.115 | convolution fusion | flops 805896192 | bytes 5832704 | tf_op jit(solution)/shard_map/dot_general | solution.py:75
  154.7 6.1 %all-to-all-start.1 = ((bf16[8,48,2048]{2,1,0:T(8,128)(2,1)}), bf16[8,48,2048]{2,1,0:T(8,128)(2,1)S(1)}, u32[]{:S(2)}, u32[]{:S(2)}) async-start(bf16[8,48,2048]{2,1,0:T(8,128)(2,1)} %bitcast.159), calls=%async_computation.1 | async-start | bytes 3145728 | tf_op jit(solution)/shard_map/all_to_all | solution.py:165
  160.8 4.9 %convolution_convert_fusion.3 = bf16[256,4096]{1,0:T(8,128)(2,1)} fusion(bf16[256,512]{1,0:T(8,128)(2,1)S(1)} %bitcast.167, bf16[512,4096]{1,0:T(8,128)(2,1)} %param.23), kind=kOutput, calls=%fused_computation.8 | convolution fusion | flops 1074790400 | bytes 6553600 | tf_op jit(solution)/shard_map/dot_general | solution.py:47
  178.1 20.0 %all-to-all-done.1 = bf16[8,48,2048]{2,1,0:T(8,128)(2,1)S(1)} async-done(((bf16[8,48,2048]{2,1,0:T(8,128)(2,1)}), bf16[8,48,2048]{2,1,0:T(8,128)(2,1)S(1)}, u32[]{:S(2)}, u32[]{:S(2)}) %all-to-all-start.1) | async-done | bytes 1572896 | tf_op jit(solution)/shard_map/all_to_all | solution.py:165
  198.1 4.3 %all-to-all-start.2 = ((bf16[8,48,2048]{2,1,0:T(8,128)(2,1)}), bf16[8,48,2048]{2,1,0:T(8,128)(2,1)}, u32[]{:S(2)}, u32[]{:S(2)}) async-start(bf16[8,48,2048]{2,1,0:T(8,128)(2,1)} %bitcast.160), calls=%async_computation.2 | async-start | bytes 3145728 | tf_op jit(solution)/shard_map/all_to_all | solution.py:165
  209.2 20.4 %collective-permute-done.2 = bf16[1,128,4096]{2,1,0:T(8,128)(2,1)} collective-permute-done((bf16[1,128,4096]{2,1,0:T(8,128)(2,1)}, bf16[1,128,4096]{2,1,0:T(8,128)(2,1)}, u32[]{:S(2)}, u32[]{:S(2)}) %collective-permute-start.2) | collective-permute-done | bytes 1048608 | tf_op jit(solution)/shard_map/ppermute | solution.py:18
  229.6 3.0 %fusion.17 = bf16[128,4096]{1,0:T(8,128)(2,1)} fusion(bf16[1,128,4096]{2,1,0:T(8,128)(2,1)} %collective-permute-done.2, bf16[1,2,128,4096]{3,2,1,0:T(8,128)(2,1)} %bitcast.35, s32[]{:T(128)S(6)} %select_n.50, bf16[1,2,128,4096]{3,2,1,0:T(8,128)(2,1)S(1)} %bitcast.163), kind=kLoop, calls=%fused_computation.34 | loop fusion | flops 3145728 | bytes 4194308 | tf_op jit(solution)/shard_map/convert_element_type | solution.py:151
  234.1 5.0 %all-to-all-done.2 = bf16[8,48,2048]{2,1,0:T(8,128)(2,1)} async-done(((bf16[8,48,2048]{2,1,0:T(8,128)(2,1)}), bf16[8,48,2048]{2,1,0:T(8,128)(2,1)}, u32[]{:S(2)}, u32[]{:S(2)}) %all-to-all-start.2) | async-done | bytes 1572896 | tf_op jit(solution)/shard_map/all_to_all | solution.py:165
  (115 shorter events, 47.4 us)
Async XLA Ops:
  0.6 31.0 %copy-start = (bf16[256,4096]{1,0:T(8,128)(2,1)S(1)}, bf16[256,4096]{1,0:T(8,128)(2,1)}, u32[]{:S(2)}) copy-start(bf16[256,4096]{1,0:T(8,128)(2,1)} %param.33) | copy-start | bytes 6291460
  0.6 119.2 %collective-permute-start.5 = (bf16[4096,256]{1,0:T(8,128)(2,1)}, bf16[4096,256]{1,0:T(8,128)(2,1)}, u32[]{:S(2)}, u32[]{:S(2)}) collective-permute-start(bf16[4096,256]{1,0:T(8,128)(2,1)} %bitcast.201), channel_id=1, source_target_pairs={{0,2},{1,3},{2,0},{3,1},{4,6},{5,7},{6,4},{7,5},{8,10},{9,11},{10,... | collective-permute-start | bytes 6291464 | tf_op jit(solution)/shard_map/ppermute | solution.py:18
  3.7 123.9 %collective-permute-start.8 = (bf16[4096,256]{1,0:T(8,128)(2,1)}, bf16[4096,256]{1,0:T(8,128)(2,1)}, u32[]{:S(2)}, u32[]{:S(2)}) collective-permute-start(bf16[4096,256]{1,0:T(8,128)(2,1)} %bitcast.202), channel_id=1, source_target_pairs={{0,1},{1,0},{2,3},{3,2},{4,5},{5,4},{6,7},{7,6},{8,9},{9,8},{10,11... | collective-permute-start | bytes 6291464 | tf_op jit(solution)/shard_map/ppermute | solution.py:18
  3.7 131.0 %collective-permute-start.6 = (bf16[4096,256]{1,0:T(8,128)(2,1)}, bf16[4096,256]{1,0:T(8,128)(2,1)}, u32[]{:S(2)}, u32[]{:S(2)}) collective-permute-start(bf16[4096,256]{1,0:T(8,128)(2,1)} %bitcast.203), channel_id=1, source_target_pairs={{0,2},{1,3},{2,0},{3,1},{4,6},{5,7},{6,4},{7,5},{8,10},{9,11},{10,... | collective-permute-start | bytes 6291464 | tf_op jit(solution)/shard_map/ppermute | solution.py:18
  3.8 139.6 %collective-permute-start.9 = (bf16[4096,256]{1,0:T(8,128)(2,1)}, bf16[4096,256]{1,0:T(8,128)(2,1)}, u32[]{:S(2)}, u32[]{:S(2)}) collective-permute-start(bf16[4096,256]{1,0:T(8,128)(2,1)} %bitcast.204), channel_id=1, source_target_pairs={{0,1},{1,0},{2,3},{3,2},{4,5},{5,4},{6,7},{7,6},{8,9},{9,8},{10,11... | collective-permute-start | bytes 6291464 | tf_op jit(solution)/shard_map/ppermute | solution.py:18
  10.8 109.7 %all-to-all-start = ((bf16[8,48,4096]{2,1,0:T(8,128)(2,1)}), bf16[8,48,4096]{2,1,0:T(8,128)(2,1)}, u32[]{:S(2)}, u32[]{:S(2)}) async-start(bf16[8,48,4096]{2,1,0:T(8,128)(2,1)} %bitcast.153), calls=%async_computation | async-start | bytes 6291456 | tf_op jit(solution)/shard_map/all_to_all | solution.py:127
  18.4 25.2 %collective-permute-start = (bf16[30,512]{1,0:T(8,128)(2,1)S(1)}, bf16[30,512]{1,0:T(8,128)(2,1)S(1)}, u32[]{:S(2)}, u32[]{:S(2)}) collective-permute-start(bf16[30,512]{1,0:T(8,128)(2,1)S(1)} %slice.288), channel_id=1, source_target_pairs={{0,4},{4,8},{8,12},{12,16},{16,20},{20,24},{24,28},{1,5},{5,9},{9,... | collective-permute-start | bytes 92168 | tf_op jit(solution)/shard_map/ppermute | solution.py:13
  43.6 99.3 %collective-permute-start.7 = (bf16[256,2048]{1,0:T(8,128)(2,1)}, bf16[256,2048]{1,0:T(8,128)(2,1)}, u32[]{:S(2)}, u32[]{:S(2)}) collective-permute-start(bf16[256,2048]{1,0:T(8,128)(2,1)} %get-tuple-element.7), channel_id=1, source_target_pairs={{0,2},{1,3},{2,0},{3,1},{4,6},{5,7},{6,4},{7,5},{8,10},{9,11},{10,... | collective-permute-start | bytes 3145736 | tf_op jit(solution)/shard_map/ppermute | solution.py:18
  45.2 74.7 %copy-start.16 = (f32[512]{0:T(512)S(1)}, f32[512]{0:T(512)}, u32[]{:S(2)}) copy-start(f32[512]{0:T(512)} %param.22) | copy-start | bytes 6148
  45.2 74.7 %copy-start.17 = (f32[512]{0:T(512)S(1)}, f32[512]{0:T(512)}, u32[]{:S(2)}) copy-start(f32[512]{0:T(512)} %param.21) | copy-start | bytes 6148
  119.9 15.2 %collective-permute-start.11 = (bf16[4096,256]{1,0:T(8,128)(2,1)}, bf16[4096,256]{1,0:T(8,128)(2,1)}, u32[]{:S(2)}, u32[]{:S(2)}) collective-permute-start(bf16[4096,256]{1,0:T(8,128)(2,1)} %collective-permute-done.5), channel_id=1, source_target_pairs={{0,1},{1,0},{2,3},{3,2},{4,5},{5,4},{6,7},{7,6},{8,9},{9,8},{10,11... | collective-permute-start | bytes 6291464 | tf_op jit(solution)/shard_map/ppermute | solution.py:18
  127.6 21.2 %collective-permute-start.10 = (bf16[256,2048]{1,0:T(8,128)(2,1)S(1)}, bf16[256,2048]{1,0:T(8,128)(2,1)S(1)}, u32[]{:S(2)}, u32[]{:S(2)}) collective-permute-start(bf16[256,2048]{1,0:T(8,128)(2,1)S(1)} %copy-done.11), channel_id=1, source_target_pairs={{0,1},{1,0},{2,3},{3,2},{4,5},{5,4},{6,7},{7,6},{8,9},{9,8},{10,11... | collective-permute-start | bytes 3145736 | tf_op jit(solution)/shard_map/ppermute | solution.py:18
  134.7 33.7 %collective-permute-start.14 = (bf16[256,2048]{1,0:T(8,128)(2,1)}, bf16[256,2048]{1,0:T(8,128)(2,1)}, u32[]{:S(2)}, u32[]{:S(2)}) collective-permute-start(bf16[256,2048]{1,0:T(8,128)(2,1)} %get-tuple-element.8), channel_id=1, source_target_pairs={{0,2},{1,3},{2,0},{3,1},{4,6},{5,7},{6,4},{7,5},{8,10},{9,11},{10,... | collective-permute-start | bytes 3145736 | tf_op jit(solution)/shard_map/ppermute | solution.py:18
  135.0 14.9 %collective-permute-start.12 = (bf16[4096,256]{1,0:T(8,128)(2,1)}, bf16[4096,256]{1,0:T(8,128)(2,1)S(1)}, u32[]{:S(2)}, u32[]{:S(2)}) collective-permute-start(bf16[4096,256]{1,0:T(8,128)(2,1)} %collective-permute-done.6), channel_id=1, source_target_pairs={{0,1},{1,0},{2,3},{3,2},{4,5},{5,4},{6,7},{7,6},{8,9},{9,8},{10,11... | collective-permute-start | bytes 6291464 | tf_op jit(solution)/shard_map/ppermute | solution.py:18
  142.8 31.6 %collective-permute-start.15 = (bf16[256,2048]{1,0:T(8,128)(2,1)}, bf16[256,2048]{1,0:T(8,128)(2,1)}, u32[]{:S(2)}, u32[]{:S(2)}) collective-permute-start(bf16[256,2048]{1,0:T(8,128)(2,1)} %get-tuple-element.8), channel_id=1, source_target_pairs={{0,1},{1,0},{2,3},{3,2},{4,5},{5,4},{6,7},{7,6},{8,9},{9,8},{10,11... | collective-permute-start | bytes 3145736 | tf_op jit(solution)/shard_map/ppermute | solution.py:18
  143.4 9.4 %collective-permute-start.13 = (bf16[256,2048]{1,0:T(8,128)(2,1)}, bf16[256,2048]{1,0:T(8,128)(2,1)S(1)}, u32[]{:S(2)}, u32[]{:S(2)}) collective-permute-start(bf16[256,2048]{1,0:T(8,128)(2,1)} %collective-permute-done.7), channel_id=1, source_target_pairs={{0,1},{1,0},{2,3},{3,2},{4,5},{5,4},{6,7},{7,6},{8,9},{9,8},{10,11... | collective-permute-start | bytes 3145736 | tf_op jit(solution)/shard_map/ppermute | solution.py:18
  148.9 20.0 %collective-permute-start.3 = (bf16[256,4096]{1,0:T(8,128)(2,1)}, bf16[256,4096]{1,0:T(8,128)(2,1)}, u32[]{:S(2)}, u32[]{:S(2)}) collective-permute-start(bf16[256,4096]{1,0:T(8,128)(2,1)} %convolution_convert_fusion.1), channel_id=1, source_target_pairs={{0,1},{1,0},{2,3},{3,2},{4,5},{5,4},{6,7},{7,6},{8,9},{9,8},{10,11... | collective-permute-start | bytes 6291464 | tf_op jit(solution)/shard_map/ppermute | solution.py:18
  154.7 43.3 %all-to-all-start.1 = ((bf16[8,48,2048]{2,1,0:T(8,128)(2,1)}), bf16[8,48,2048]{2,1,0:T(8,128)(2,1)S(1)}, u32[]{:S(2)}, u32[]{:S(2)}) async-start(bf16[8,48,2048]{2,1,0:T(8,128)(2,1)} %bitcast.159), calls=%async_computation.1 | async-start | bytes 3145728 | tf_op jit(solution)/shard_map/all_to_all | solution.py:165
  165.7 36.7 %collective-permute-start.1 = (bf16[256,4096]{1,0:T(8,128)(2,1)}, bf16[256,4096]{1,0:T(8,128)(2,1)}, u32[]{:S(2)}, u32[]{:S(2)}) collective-permute-start(bf16[256,4096]{1,0:T(8,128)(2,1)} %convolution_convert_fusion.3), channel_id=1, source_target_pairs={{0,1},{1,0},{2,3},{3,2},{4,5},{5,4},{6,7},{7,6},{8,9},{9,8},{10,11... | collective-permute-start | bytes 6291464 | tf_op jit(solution)/shard_map/ppermute | solution.py:18
  168.4 7.9 %collective-permute-start.16 = (bf16[256,2048]{1,0:T(8,128)(2,1)}, bf16[256,2048]{1,0:T(8,128)(2,1)S(1)}, u32[]{:S(2)}, u32[]{:S(2)}) collective-permute-start(bf16[256,2048]{1,0:T(8,128)(2,1)} %collective-permute-done.14), channel_id=1, source_target_pairs={{0,1},{1,0},{2,3},{3,2},{4,5},{5,4},{6,7},{7,6},{8,9},{9,8},{10,11... | collective-permute-start | bytes 3145736 | tf_op jit(solution)/shard_map/ppermute | solution.py:18
  170.5 36.2 %collective-permute-start.4 = (bf16[1,128,4096]{2,1,0:T(8,128)(2,1)S(1)}, bf16[1,128,4096]{2,1,0:T(8,128)(2,1)}, u32[]{:S(2)}, u32[]{:S(2)}) collective-permute-start(bf16[1,128,4096]{2,1,0:T(8,128)(2,1)S(1)} %fusion.26), channel_id=1, source_target_pairs={{0,2},{1,3},{2,0},{3,1},{4,6},{5,7},{6,4},{7,5},{8,10},{9,11},{10,... | collective-permute-start | bytes 3145736 | tf_op jit(solution)/shard_map/ppermute | solution.py:18
  198.1 34.5 %copy-start.2 = (bf16[8,48,2048]{2,1,0:T(8,128)(2,1)}, bf16[8,48,2048]{2,1,0:T(8,128)(2,1)S(1)}, u32[]{:S(2)}) copy-start(bf16[8,48,2048]{2,1,0:T(8,128)(2,1)S(1)} %all-to-all-done.1) | copy-start | bytes 4718596
  198.1 40.9 %all-to-all-start.2 = ((bf16[8,48,2048]{2,1,0:T(8,128)(2,1)}), bf16[8,48,2048]{2,1,0:T(8,128)(2,1)}, u32[]{:S(2)}, u32[]{:S(2)}) async-start(bf16[8,48,2048]{2,1,0:T(8,128)(2,1)} %bitcast.160), calls=%async_computation.2 | async-start | bytes 3145728 | tf_op jit(solution)/shard_map/all_to_all | solution.py:165
  205.2 24.4 %collective-permute-start.2 = (bf16[1,128,4096]{2,1,0:T(8,128)(2,1)}, bf16[1,128,4096]{2,1,0:T(8,128)(2,1)}, u32[]{:S(2)}, u32[]{:S(2)}) collective-permute-start(bf16[1,128,4096]{2,1,0:T(8,128)(2,1)} %fusion.25), channel_id=1, source_target_pairs={{0,2},{1,3},{2,0},{3,1},{4,6},{5,7},{6,4},{7,5},{8,10},{9,11},{10,... | collective-permute-start | bytes 3145736 | tf_op jit(solution)/shard_map/ppermute | solution.py:18
  (18 other events, 90.2 us)

commit v2 on v1

--- a/solution.py
+++ b/solution.py
@@ -104,10 +104,6 @@
     gates = gathered(expert_gate[0], "tp")
     ups = gathered(expert_up[0], "tp")
     chunk = model_width // COLUMN_CHUNKS
-    downs = [
-        gathered(expert_down[0][:, c * chunk : (c + 1) * chunk], "tp")
-        for c in range(COLUMN_CHUNKS)
-    ]
 
     own = lax.dynamic_slice_in_dim(tokens_b, lax.axis_index("tp") * rows_own, rows_own, 0)
     own_rows = rms_normed(own, norm_gain)
@@ -138,29 +134,22 @@
     filtered = jnp.zeros(gated.shape, jnp.float32) + conv_bias[None, :]
     for tap_index in range(rim_rows + 1):
         filtered = filtered + conv_taps[tap_index][None, :] * padded[tap_index : tap_index + length]
-    row_sum, squares = lax.psum(
-        (jnp.sum(filtered, axis=1), jnp.sum(filtered * filtered, axis=1)), "tp"
-    )
-    channel_count = filtered.shape[1] * tp_count
-    average = row_sum / channel_count
-    variance = squares / channel_count - average * average
-    normed_a = (filtered - average[:, None]) * lax.rsqrt(
-        variance[:, None] + EPSILON
-    ) * ln_gain + ln_bias
-    activated = jax.nn.silu(normed_a).astype(jnp.bfloat16)
-    mixer_rows = scattered_product(activated, out_proj, "tp").astype(jnp.bfloat16)
-
     normed_b = rms_normed(tokens_b, norm_gain)
     hidden_shared = gated_hidden(normed_b, shared_gate, shared_up)
     shared_rows = scattered_product(hidden_shared, shared_down, "tp").astype(jnp.bfloat16)
 
     hidden = [gated_hidden(arrived, g, u) for g, u in zip(gates, ups)]
-    parts = []
-    for pieces in downs:
+    parts, products = [], []
+    for c in range(COLUMN_CHUNKS):
+        local = expert_down[0][:, c * chunk : (c + 1) * chunk]
+        if products:
+            local, _ = lax.optimization_barrier((local, products[-1]))
+        pieces = gathered(local, "tp")
         product = sum(
             jnp.dot(h, piece, preferred_element_type=jnp.float32)
             for h, piece in zip(hidden, pieces)
         ).astype(jnp.bfloat16)
+        products.append(product)
         parts.append(
             lax.all_to_all(
                 product.reshape(ep_count, capacity, chunk),
@@ -170,6 +159,19 @@
                 tiled=True,
             ).reshape(ep_count * capacity, chunk)
         )
+    row_sum, squares, _ = lax.optimization_barrier(
+        (jnp.sum(filtered, axis=1), jnp.sum(filtered * filtered, axis=1), products[0])
+    )
+    row_sum, squares = lax.psum((row_sum, squares), "tp")
+    channel_count = filtered.shape[1] * tp_count
+    average = row_sum / channel_count
+    variance = squares / channel_count - average * average
+    normed_a = (filtered - average[:, None]) * lax.rsqrt(
+        variance[:, None] + EPSILON
+    ) * ln_gain + ln_bias
+    activated = jax.nn.silu(normed_a).astype(jnp.bfloat16)
+    mixer_rows = scattered_product(activated, out_proj, "tp").astype(jnp.bfloat16)
+
     outs = []
     for c, returned in enumerate(parts):
         total = shared_rows[:, c * chunk : (c + 1) * chunk].astype(jnp.float32)

time: 246 us -> 237 us (0.963)
  blocking collectives: 69.6 us -> 26.6 us
  waiting for transfers between devices: 51.6 us -> 87.6 us
  matrix products: 65.6 us -> 63 us
    psum x1, blocking collectives: 69.6 us -> 26.6 us  [per_device(): row_sum, squares = lax.psum((row_sum, squares), 'tp')]
    all_to_all x1, waiting for transfers between devices: 0.01 us -> 32.3 us  [per_device(): lax.all_to_all(outbox.reshape(ep_count, capacity, model_width), 'ep', spl...]
    ppermute x16, waiting for transfers between devices: 20.5 us -> 46.1 us  [swapped(): return lax.ppermute(x, axis, [(i, i ^ bit) for i in range(devices)])]
    all_to_all x2, waiting for transfers between devices: 24.9 us -> 2.11 us  [per_device(): lax.all_to_all(product.reshape(ep_count, capacity, chunk), 'ep', split_ax...]
  transfers between devices with their start and end apart: 20 -> 20, of which waited for: 4 -> 7; matrix products, arithmetic and copies ran while one was open for 35% -> 35% of each run, Pallas kernels for 0% -> 0%
where the time goes in v2:
time: 237 us; the launch traced here: 236 us
  waiting for transfers between devices  87.6 us (37%)
  matrix products  63 us (27%)
  starting transfers between devices  31.6 us (13%)
  blocking collectives  26.6 us (11%)
  other arithmetic  22.9 us (10%)
  local copies, waits for them, and re-layouts  3.3 us (1%)
    ppermute x16, waiting for transfers between devices, swapped(): return lax.ppermute(x, axis, [(i, i ^ bit) for i in range(devices)])  46.1 us
    all_to_all x1, waiting for transfers between devices, per_device(): lax.all_to_all(outbox.reshape(ep_count, capacity, model_width), 'ep', spl...  32.3 us
    psum x1, blocking collectives, per_device(): row_sum, squares = lax.psum((row_sum, squares), 'tp')  26.6 us
    dot_general x5, matrix products, gated_hidden(): jnp.dot(rows_in, weight_gate, preferred_element_type=jnp.float32)  17.2 us
    dot_general x5, matrix products, gated_hidden(): jnp.dot(rows_in, weight_up, preferred_element_type=jnp.float32)  14.3 us
    all_to_all x2, starting transfers between devices, per_device(): lax.all_to_all(product.reshape(ep_count, capacity, chunk), 'ep', split_ax...  11.9 us
    dot_general x8, matrix products, per_device(): jnp.dot(h, piece, preferred_element_type=jnp.float32)  9.64 us
    ppermute x16, starting transfers between devices, swapped(): return lax.ppermute(x, axis, [(i, i ^ bit) for i in range(devices)])  9.51 us
  transfers between devices with their start and end apart: 20, of which 7 were waited for; matrix products, arithmetic and copies ran while one was open for 35% of the time, Pallas kernels for 0%

profile of v2, /device:TPU:0, one launch (start us, length us, event | category | flops | bytes accessed | tf_op | source)
XLA Modules:
  0.0 236.2 jit_solution(6657440936348305720)
XLA Ops:
  0.6 3.0 %collective-permute-start.1 = (bf16[4096,256]{1,0:T(8,128)(2,1)}, bf16[4096,256]{1,0:T(8,128)(2,1)}, u32[]{:S(2)}, u32[]{:S(2)}) collective-permute-start(bf16[4096,256]{1,0:T(8,128)(2,1)} %bitcast.201), channel_id=1, source_target_pairs={{0,2},{1,3},{2,0},{3,1},{4,6},{5,7},{6,4},{7,5},{8,10},{9,11},{10,... | collective-permute-start | bytes 6291464 | tf_op jit(solution)/shard_map/ppermute | solution.py:18
  6.8 4.0 %convolution_convert_fusion = bf16[384,4096]{1,0:T(8,128)(2,1)} fusion(pred[384,128]{1,0:T(32,128)(4,1)S(1)} %fusion.68, f32[4096]{0:T(1024)} %param.25, f32[128]{0:T(128)S(1)} %add_rsqrt_fusion.2, bf16[512,4096]{1,0:T(8,128)(2,1)} %param.24, s32[]{:T(128)S(6)} %select_n.46), kind=kOutput, calls=%fused_computation.5 | convolution fusion | flops 406323200 | bytes 4260356 | tf_op jit(solution)/shard_map/dot_general | solution.py:122
  10.8 6.2 %all-to-all-start = ((bf16[8,48,4096]{2,1,0:T(8,128)(2,1)}), bf16[8,48,4096]{2,1,0:T(8,128)(2,1)}, u32[]{:S(2)}, u32[]{:S(2)}) async-start(bf16[8,48,4096]{2,1,0:T(8,128)(2,1)} %bitcast.154), calls=%async_computation | async-start | bytes 6291456 | tf_op jit(solution)/shard_map/all_to_all | solution.py:123
  18.4 3.9 %collective-permute-start = (bf16[30,512]{1,0:T(8,128)(2,1)S(1)}, bf16[30,512]{1,0:T(8,128)(2,1)S(1)}, u32[]{:S(2)}, u32[]{:S(2)}) collective-permute-start(bf16[30,512]{1,0:T(8,128)(2,1)S(1)} %slice.288), channel_id=1, source_target_pairs={{0,4},{4,8},{8,12},{12,16},{16,20},{20,24},{24,28},{1,5},{5,9},{9,... | collective-permute-start | bytes 92168 | tf_op jit(solution)/shard_map/ppermute | solution.py:13
  22.3 3.2 %fusion = f32[512]{0:T(512)S(1)} fusion(bf16[512,4096]{1,0:T(8,128)(2,1)} %param.24), kind=kLoop, calls=%fused_computation.2 | loop fusion | flops 6290944 | bytes 4196352 | tf_op jit(solution)/shard_map/reduce_sum | solution.py:67
  25.8 3.0 %fusion.19 = f32[512,256]{1,0:T(8,128)S(1)} fusion(bf16[4096,256]{1,0:T(8,128)(2,1)} %param.31, bf16[512,4096]{1,0:T(8,128)(2,1)S(1)} %copy-done.2, f32[4096]{0:T(1024)S(1)} %copy-done.16, f32[512]{0:T(512)S(1)} %add_rsqrt_fusion), kind=kOutput, calls=%fused_computation.38 | convolution fusion | flops 1082130432 | bytes 6834176 | tf_op jit(solution)/shard_map/dot_general | solution.py:74
  36.5 7.0 %collective-permute-done = bf16[30,512]{1,0:T(8,128)(2,1)S(1)} collective-permute-done((bf16[30,512]{1,0:T(8,128)(2,1)S(1)}, bf16[30,512]{1,0:T(8,128)(2,1)S(1)}, u32[]{:S(2)}, u32[]{:S(2)}) %collective-permute-start) | collective-permute-done | bytes 30752 | tf_op jit(solution)/shard_map/ppermute | solution.py:13
  45.2 5.2 %collective-permute-done.1 = bf16[4096,256]{1,0:T(8,128)(2,1)} collective-permute-done((bf16[4096,256]{1,0:T(8,128)(2,1)}, bf16[4096,256]{1,0:T(8,128)(2,1)}, u32[]{:S(2)}, u32[]{:S(2)}) %collective-permute-start.1) | collective-permute-done | bytes 2097184 | tf_op jit(solution)/shard_map/ppermute | solution.py:18
  50.5 5.5 %multiply_reduce_fusion = (f32[512]{0:T(512)S(1)}, f32[512]{0:T(512)}, f32[512,512]{1,0:T(8,128)S(1)}) fusion(f32[542,512]{1,0:T(8,128)S(1)} %maximum_convert_fusion, f32[512]{0:T(512)S(1)} %bitcast.179, f32[512]{0:T(512)S(1)} %bitcast.180, f32[512]{0:T(512)S(1)} %bitcast.182, f32[512]{0:T(512)S(1)} %bitcast.183, f32[512]{0:T(512)S(1)} %bitcast.184, ...), kind=kLoop, calls=%fused_computation.111 | loop fusion | flops 17038336 | bytes 33624064 | tf_op jit(solution)/shard_map/reduce_sum | solution.py:163
  55.9 32.3 %all-to-all-done = bf16[8,48,4096]{2,1,0:T(8,128)(2,1)} async-done(((bf16[8,48,4096]{2,1,0:T(8,128)(2,1)}), bf16[8,48,4096]{2,1,0:T(8,128)(2,1)}, u32[]{:S(2)}, u32[]{:S(2)}) %all-to-all-start) | async-done | bytes 3145760 | tf_op jit(solution)/shard_map/all_to_all | solution.py:123
  88.2 3.5 %fusion.79 = f32[384,256]{1,0:T(8,128)S(1)} fusion(bf16[384,4096]{1,0:T(8,128)(2,1)} %bitcast.35, bf16[1,4096,256]{2,1,0:T(8,128)(2,1)} %param.28), kind=kOutput, calls=%fused_computation.147 | convolution fusion | flops 805306368 | bytes 5636096 | tf_op jit(solution)/shard_map/dot_general | solution.py:74
  91.8 3.5 %fusion.88 = f32[384,256]{1,0:T(8,128)S(1)} fusion(bf16[384,4096]{1,0:T(8,128)(2,1)} %bitcast.35, bf16[4096,256]{1,0:T(8,128)(2,1)} %collective-permute-done.1), kind=kOutput, calls=%fused_computation.155 | convolution fusion | flops 805306368 | bytes 5636096 | tf_op jit(solution)/shard_map/dot_general | solution.py:74
  95.4 3.6 %fusion.90 = f32[384,256]{1,0:T(8,128)S(1)} fusion(bf16[384,4096]{1,0:T(8,128)(2,1)} %bitcast.35, bf16[4096,256]{1,0:T(8,128)(2,1)} %collective-permute-done.4), kind=kOutput, calls=%fused_computation.157 | convolution fusion | flops 805306368 | bytes 5636096 | tf_op jit(solution)/shard_map/dot_general | solution.py:74
  99.1 2.9 %fusion.24 = bf16[384,256]{1,0:T(8,128)(2,1)S(1)} fusion(bf16[384,4096]{1,0:T(8,128)(2,1)} %bitcast.35, f32[384,256]{1,0:T(8,128)S(1)} %fusion.79, bf16[1,4096,256]{2,1,0:T(8,128)(2,1)S(1)} %copy-done.24), kind=kOutput, calls=%fused_computation.41 | convolution fusion | flops 805896192 | bytes 5832704 | tf_op jit(solution)/shard_map/dot_general | solution.py:75
  102.0 15.1 %collective-permute-done.3 = bf16[256,2048]{1,0:T(8,128)(2,1)} collective-permute-done((bf16[256,2048]{1,0:T(8,128)(2,1)}, bf16[256,2048]{1,0:T(8,128)(2,1)}, u32[]{:S(2)}, u32[]{:S(2)}) %collective-permute-start.3) | collective-permute-done | bytes 1048608 | tf_op jit(solution)/shard_map/ppermute | solution.py:18
  117.6 3.5 %fusion.92 = f32[384,256]{1,0:T(8,128)S(1)} fusion(bf16[384,4096]{1,0:T(8,128)(2,1)} %bitcast.35, bf16[4096,256]{1,0:T(8,128)(2,1)} %collective-permute-done.7), kind=kOutput, calls=%fused_computation.159 | convolution fusion | flops 805306368 | bytes 5636096 | tf_op jit(solution)/shard_map/dot_general | solution.py:74
  121.2 3.7 %multiply_convert_fusion.4 = bf16[384,256]{1,0:T(8,128)(2,1)S(1)} fusion(f32[384,256]{1,0:T(8,128)S(1)} %fusion.88, bf16[384,4096]{1,0:T(8,128)(2,1)} %bitcast.35, bf16[4096,256]{1,0:T(8,128)(2,1)} %collective-permute-done.2), kind=kOutput, calls=%fused_computation.117 | convolution fusion | flops 805896192 | bytes 5832704 | tf_op jit(solution)/shard_map/dot_general | solution.py:75
  125.5 3.5 %multiply_convert_fusion.3 = bf16[384,256]{1,0:T(8,128)(2,1)S(1)} fusion(f32[384,256]{1,0:T(8,128)S(1)} %fusion.90, bf16[384,4096]{1,0:T(8,128)(2,1)} %bitcast.35, bf16[4096,256]{1,0:T(8,128)(2,1)} %collective-permute-done.5), kind=kOutput, calls=%fused_computation.116 | convolution fusion | flops 805896192 | bytes 5832704 | tf_op jit(solution)/shard_map/dot_general | solution.py:75
  136.2 6.2 %all-to-all-start.1 = ((bf16[8,48,2048]{2,1,0:T(8,128)(2,1)}), bf16[8,48,2048]{2,1,0:T(8,128)(2,1)S(1)}, u32[]{:S(2)}, u32[]{:S(2)}) async-start(bf16[8,48,2048]{2,1,0:T(8,128)(2,1)} %bitcast.157), calls=%async_computation.1 | async-start | bytes 3145728 | tf_op jit(solution)/shard_map/all_to_all | solution.py:154
  143.9 26.6 %all-reduce = (f32[512]{0:T(512)S(1)}, f32[512]{0:T(512)S(1)}) all-reduce(f32[512]{0:T(512)S(1)} %get-tuple-element.6, f32[512]{0:T(512)S(1)} %copy-done.17), channel_id=1, replica_groups=mesh['ep'=8,'tp'=4] {'tp'}, use_global_device_ids=true, to_apply=%region_5.6 | all-reduce | flops 1024 | bytes 8192 | tf_op jit(solution)/shard_map/psum | solution.py:165
  171.7 5.0 %convolution_convert_fusion.3 = bf16[256,4096]{1,0:T(8,128)(2,1)} fusion(bf16[256,512]{1,0:T(8,128)(2,1)S(1)} %bitcast.167, bf16[512,4096]{1,0:T(8,128)(2,1)} %param.23), kind=kOutput, calls=%fused_computation.8 | convolution fusion | flops 1074790400 | bytes 6553600 | tf_op jit(solution)/shard_map/dot_general | solution.py:47
  187.7 5.7 %all-to-all-start.2 = ((bf16[8,48,2048]{2,1,0:T(8,128)(2,1)}), bf16[8,48,2048]{2,1,0:T(8,128)(2,1)}, u32[]{:S(2)}, u32[]{:S(2)}) async-start(bf16[8,48,2048]{2,1,0:T(8,128)(2,1)} %bitcast.158), calls=%async_computation.2 | async-start | bytes 3145728 | tf_op jit(solution)/shard_map/all_to_all | solution.py:154
  196.5 8.0 %collective-permute-done.13 = bf16[1,128,4096]{2,1,0:T(8,128)(2,1)} collective-permute-done((bf16[1,128,4096]{2,1,0:T(8,128)(2,1)S(1)}, bf16[1,128,4096]{2,1,0:T(8,128)(2,1)}, u32[]{:S(2)}, u32[]{:S(2)}) %collective-permute-start.13) | collective-permute-done | bytes 1048608 | tf_op jit(solution)/shard_map/ppermute | solution.py:18
  208.4 17.8 %collective-permute-done.11 = bf16[1,128,4096]{2,1,0:T(8,128)(2,1)S(1)} collective-permute-done((bf16[1,128,4096]{2,1,0:T(8,128)(2,1)S(1)}, bf16[1,128,4096]{2,1,0:T(8,128)(2,1)S(1)}, u32[]{:S(2)}, u32[]{:S(2)}) %collective-permute-start.11) | collective-permute-done | bytes 1048608 | tf_op jit(solution)/shard_map/ppermute | solution.py:18
  (121 shorter events, 52.9 us)
Async XLA Ops:
  0.6 29.7 %copy-start = (bf16[256,4096]{1,0:T(8,128)(2,1)S(1)}, bf16[256,4096]{1,0:T(8,128)(2,1)}, u32[]{:S(2)}) copy-start(bf16[256,4096]{1,0:T(8,128)(2,1)} %param.33) | copy-start | bytes 6291460
  0.6 49.8 %collective-permute-start.1 = (bf16[4096,256]{1,0:T(8,128)(2,1)}, bf16[4096,256]{1,0:T(8,128)(2,1)}, u32[]{:S(2)}, u32[]{:S(2)}) collective-permute-start(bf16[4096,256]{1,0:T(8,128)(2,1)} %bitcast.201), channel_id=1, source_target_pairs={{0,2},{1,3},{2,0},{3,1},{4,6},{5,7},{6,4},{7,5},{8,10},{9,11},{10,... | collective-permute-start | bytes 6291464 | tf_op jit(solution)/shard_map/ppermute | solution.py:18
  3.7 91.6 %collective-permute-start.4 = (bf16[4096,256]{1,0:T(8,128)(2,1)}, bf16[4096,256]{1,0:T(8,128)(2,1)}, u32[]{:S(2)}, u32[]{:S(2)}) collective-permute-start(bf16[4096,256]{1,0:T(8,128)(2,1)} %bitcast.202), channel_id=1, source_target_pairs={{0,1},{1,0},{2,3},{3,2},{4,5},{5,4},{6,7},{7,6},{8,9},{9,8},{10,11... | collective-permute-start | bytes 6291464 | tf_op jit(solution)/shard_map/ppermute | solution.py:18
  3.7 113.4 %collective-permute-start.2 = (bf16[4096,256]{1,0:T(8,128)(2,1)}, bf16[4096,256]{1,0:T(8,128)(2,1)}, u32[]{:S(2)}, u32[]{:S(2)}) collective-permute-start(bf16[4096,256]{1,0:T(8,128)(2,1)} %bitcast.203), channel_id=1, source_target_pairs={{0,2},{1,3},{2,0},{3,1},{4,6},{5,7},{6,4},{7,5},{8,10},{9,11},{10,... | collective-permute-start | bytes 6291464 | tf_op jit(solution)/shard_map/ppermute | solution.py:18
  3.8 121.6 %collective-permute-start.5 = (bf16[4096,256]{1,0:T(8,128)(2,1)}, bf16[4096,256]{1,0:T(8,128)(2,1)}, u32[]{:S(2)}, u32[]{:S(2)}) collective-permute-start(bf16[4096,256]{1,0:T(8,128)(2,1)} %bitcast.204), channel_id=1, source_target_pairs={{0,1},{1,0},{2,3},{3,2},{4,5},{5,4},{6,7},{7,6},{8,9},{9,8},{10,11... | collective-permute-start | bytes 6291464 | tf_op jit(solution)/shard_map/ppermute | solution.py:18
  10.8 77.5 %all-to-all-start = ((bf16[8,48,4096]{2,1,0:T(8,128)(2,1)}), bf16[8,48,4096]{2,1,0:T(8,128)(2,1)}, u32[]{:S(2)}, u32[]{:S(2)}) async-start(bf16[8,48,4096]{2,1,0:T(8,128)(2,1)} %bitcast.154), calls=%async_computation | async-start | bytes 6291456 | tf_op jit(solution)/shard_map/all_to_all | solution.py:123
  18.4 25.2 %collective-permute-start = (bf16[30,512]{1,0:T(8,128)(2,1)S(1)}, bf16[30,512]{1,0:T(8,128)(2,1)S(1)}, u32[]{:S(2)}, u32[]{:S(2)}) collective-permute-start(bf16[30,512]{1,0:T(8,128)(2,1)S(1)} %slice.288), channel_id=1, source_target_pairs={{0,4},{4,8},{8,12},{12,16},{16,20},{20,24},{24,28},{1,5},{5,9},{9,... | collective-permute-start | bytes 92168 | tf_op jit(solution)/shard_map/ppermute | solution.py:13
  34.6 15.9 %copy-start.20 = (f32[512]{0:T(512)S(1)}, f32[512]{0:T(512)}, u32[]{:S(2)}) copy-start(f32[512]{0:T(512)} %param.20) | copy-start | bytes 6148
  43.6 73.5 %collective-permute-start.3 = (bf16[256,2048]{1,0:T(8,128)(2,1)}, bf16[256,2048]{1,0:T(8,128)(2,1)}, u32[]{:S(2)}, u32[]{:S(2)}) collective-permute-start(bf16[256,2048]{1,0:T(8,128)(2,1)} %get-tuple-element.14), channel_id=1, source_target_pairs={{0,2},{1,3},{2,0},{3,1},{4,6},{5,7},{6,4},{7,5},{8,10},{9,11},{10,... | collective-permute-start | bytes 3145736 | tf_op jit(solution)/shard_map/ppermute | solution.py:18
  50.5 67.1 %collective-permute-start.7 = (bf16[4096,256]{1,0:T(8,128)(2,1)}, bf16[4096,256]{1,0:T(8,128)(2,1)}, u32[]{:S(2)}, u32[]{:S(2)}) collective-permute-start(bf16[4096,256]{1,0:T(8,128)(2,1)} %collective-permute-done.1), channel_id=1, source_target_pairs={{0,1},{1,0},{2,3},{3,2},{4,5},{5,4},{6,7},{7,6},{8,9},{9,8},{10,11... | collective-permute-start | bytes 6291464 | tf_op jit(solution)/shard_map/ppermute | solution.py:18
  95.3 35.5 %collective-permute-start.6 = (bf16[256,2048]{1,0:T(8,128)(2,1)}, bf16[256,2048]{1,0:T(8,128)(2,1)S(1)}, u32[]{:S(2)}, u32[]{:S(2)}) collective-permute-start(bf16[256,2048]{1,0:T(8,128)(2,1)} %get-tuple-element.14), channel_id=1, source_target_pairs={{0,1},{1,0},{2,3},{3,2},{4,5},{5,4},{6,7},{7,6},{8,9},{9,8},{10,11... | collective-permute-start | bytes 3145736 | tf_op jit(solution)/shard_map/ppermute | solution.py:18
  102.0 22.9 %copy-start.10 = (bf16[384,256]{1,0:T(8,128)(2,1)}, bf16[384,256]{1,0:T(8,128)(2,1)S(1)}, u32[]{:S(2)}) copy-start(bf16[384,256]{1,0:T(8,128)(2,1)S(1)} %fusion.24) | copy-start | bytes 589828
  117.0 59.6 %collective-permute-start.12 = (bf16[256,4096]{1,0:T(8,128)(2,1)}, bf16[256,4096]{1,0:T(8,128)(2,1)}, u32[]{:S(2)}, u32[]{:S(2)}) collective-permute-start(bf16[256,4096]{1,0:T(8,128)(2,1)} %convolution_convert_fusion.1), channel_id=1, source_target_pairs={{0,1},{1,0},{2,3},{3,2},{4,5},{5,4},{6,7},{7,6},{8,9},{9,8},{10,11... | collective-permute-start | bytes 6291464 | tf_op jit(solution)/shard_map/ppermute | solution.py:18
  117.0 17.2 %collective-permute-start.9 = (bf16[256,2048]{1,0:T(8,128)(2,1)}, bf16[256,2048]{1,0:T(8,128)(2,1)S(1)}, u32[]{:S(2)}, u32[]{:S(2)}) collective-permute-start(bf16[256,2048]{1,0:T(8,128)(2,1)} %collective-permute-done.3), channel_id=1, source_target_pairs={{0,1},{1,0},{2,3},{3,2},{4,5},{5,4},{6,7},{7,6},{8,9},{9,8},{10,11... | collective-permute-start | bytes 3145736 | tf_op jit(solution)/shard_map/ppermute | solution.py:18
  117.6 13.8 %collective-permute-start.8 = (bf16[4096,256]{1,0:T(8,128)(2,1)}, bf16[4096,256]{1,0:T(8,128)(2,1)S(1)}, u32[]{:S(2)}, u32[]{:S(2)}) collective-permute-start(bf16[4096,256]{1,0:T(8,128)(2,1)} %collective-permute-done.2), channel_id=1, source_target_pairs={{0,1},{1,0},{2,3},{3,2},{4,5},{5,4},{6,7},{7,6},{8,9},{9,8},{10,11... | collective-permute-start | bytes 6291464 | tf_op jit(solution)/shard_map/ppermute | solution.py:18
  136.2 51.5 %all-to-all-start.1 = ((bf16[8,48,2048]{2,1,0:T(8,128)(2,1)}), bf16[8,48,2048]{2,1,0:T(8,128)(2,1)S(1)}, u32[]{:S(2)}, u32[]{:S(2)}) async-start(bf16[8,48,2048]{2,1,0:T(8,128)(2,1)} %bitcast.157), calls=%async_computation.1 | async-start | bytes 3145728 | tf_op jit(solution)/shard_map/all_to_all | solution.py:154
  142.4 37.2 %collective-permute-start.14 = (bf16[256,2048]{1,0:T(8,128)(2,1)}, bf16[256,2048]{1,0:T(8,128)(2,1)}, u32[]{:S(2)}, u32[]{:S(2)}) collective-permute-start(bf16[256,2048]{1,0:T(8,128)(2,1)} %get-tuple-element.7), channel_id=1, source_target_pairs={{0,2},{1,3},{2,0},{3,1},{4,6},{5,7},{6,4},{7,5},{8,10},{9,11},{10,... | collective-permute-start | bytes 3145736 | tf_op jit(solution)/shard_map/ppermute | solution.py:18
  176.7 16.7 %collective-permute-start.10 = (bf16[256,4096]{1,0:T(8,128)(2,1)}, bf16[256,4096]{1,0:T(8,128)(2,1)}, u32[]{:S(2)}, u32[]{:S(2)}) collective-permute-start(bf16[256,4096]{1,0:T(8,128)(2,1)} %convolution_convert_fusion.3), channel_id=1, source_target_pairs={{0,1},{1,0},{2,3},{3,2},{4,5},{5,4},{6,7},{7,6},{8,9},{9,8},{10,11... | collective-permute-start | bytes 6291464 | tf_op jit(solution)/shard_map/ppermute | solution.py:18
  178.3 26.2 %collective-permute-start.13 = (bf16[1,128,4096]{2,1,0:T(8,128)(2,1)S(1)}, bf16[1,128,4096]{2,1,0:T(8,128)(2,1)}, u32[]{:S(2)}, u32[]{:S(2)}) collective-permute-start(bf16[1,128,4096]{2,1,0:T(8,128)(2,1)S(1)} %fusion.26), channel_id=1, source_target_pairs={{0,2},{1,3},{2,0},{3,1},{4,6},{5,7},{6,4},{7,5},{8,10},{9,11},{10,... | collective-permute-start | bytes 3145736 | tf_op jit(solution)/shard_map/ppermute | solution.py:18
  178.9 6.0 %collective-permute-start.15 = (bf16[256,2048]{1,0:T(8,128)(2,1)S(1)}, bf16[256,2048]{1,0:T(8,128)(2,1)S(1)}, u32[]{:S(2)}, u32[]{:S(2)}) collective-permute-start(bf16[256,2048]{1,0:T(8,128)(2,1)S(1)} %copy-done.7), channel_id=1, source_target_pairs={{0,1},{1,0},{2,3},{3,2},{4,5},{5,4},{6,7},{7,6},{8,9},{9,8},{10,11... | collective-permute-start | bytes 3145736 | tf_op jit(solution)/shard_map/ppermute | solution.py:18
  179.6 5.9 %collective-permute-start.16 = (bf16[256,2048]{1,0:T(8,128)(2,1)}, bf16[256,2048]{1,0:T(8,128)(2,1)S(1)}, u32[]{:S(2)}, u32[]{:S(2)}) collective-permute-start(bf16[256,2048]{1,0:T(8,128)(2,1)} %collective-permute-done.14), channel_id=1, source_target_pairs={{0,1},{1,0},{2,3},{3,2},{4,5},{5,4},{6,7},{7,6},{8,9},{9,8},{10,11... | collective-permute-start | bytes 3145736 | tf_op jit(solution)/shard_map/ppermute | solution.py:18
  187.7 43.4 %all-to-all-start.2 = ((bf16[8,48,2048]{2,1,0:T(8,128)(2,1)}), bf16[8,48,2048]{2,1,0:T(8,128)(2,1)}, u32[]{:S(2)}, u32[]{:S(2)}) async-start(bf16[8,48,2048]{2,1,0:T(8,128)(2,1)} %bitcast.158), calls=%async_computation.2 | async-start | bytes 3145728 | tf_op jit(solution)/shard_map/all_to_all | solution.py:154
  195.4 30.9 %collective-permute-start.11 = (bf16[1,128,4096]{2,1,0:T(8,128)(2,1)S(1)}, bf16[1,128,4096]{2,1,0:T(8,128)(2,1)S(1)}, u32[]{:S(2)}, u32[]{:S(2)}) collective-permute-start(bf16[1,128,4096]{2,1,0:T(8,128)(2,1)S(1)} %fusion.25), channel_id=1, source_target_pairs={{0,2},{1,3},{2,0},{3,1},{4,6},{5,7},{6,4},{7,5},{8,10},{9,11},{10,... | collective-permute-start | bytes 3145736 | tf_op jit(solution)/shard_map/ppermute | solution.py:18
  207.0 19.3 %copy-start.8 = (bf16[256,4096]{1,0:T(8,128)(2,1)S(1)}, bf16[256,4096]{1,0:T(8,128)(2,1)}, u32[]{:S(2)}) copy-start(bf16[256,4096]{1,0:T(8,128)(2,1)} %convolution_convert_fusion.4) | copy-start | bytes 6291460
  (21 other events, 86.0 us)
